TPU v7x, 512 devices: a whole 4x4x16 slice. The times are simulated.
512 devices in a mesh: sp: 32 (over z, core), tp: 16 (over y, x).
Axes of the slice: x: 4, y: 4, z: 16, core: 2. Of those that a mesh axis runs over, the one named last changes fastest.
Arguments:
- layer_input: bfloat16 [32768, 4096], P('sp', 'tp'), may hold values from -6 to 6
- key_weight: bfloat16 [4096, 4096], P(None, 'tp'), may hold values from -0.09375 to 0.09375
- value_weight: bfloat16 [4096, 4096], P(None, 'tp'), may hold values from -0.09375 to 0.09375
- decay_exponent: float32 [32], P('tp'), may hold values from -0.077 to -4.2114258e-05, as said below
- query_new: bfloat16 [2, 4096], P(None, 'tp'), may hold values from -6 to 6
- key_new: bfloat16 [2, 4096], P(None, 'tp'), may hold values from -6 to 6
- value_new: bfloat16 [2, 4096], P(None, 'tp'), may hold values from -6 to 6
- norm_gain: float32 [4096], P('tp'), may hold values from 0.1 to 1.9
Outputs:
- state_cache: bfloat16 [2, 32, 128, 128], P(None, 'tp', 'sp')
- first_read: bfloat16 [2, 4096], P(None, 'tp')
Inputs may be any that keep to these rules, and one draw needn't show every extreme that they name: decay_exponent is negative.
All inputs are finite; a program needn't handle non-finite values.
Results may differ from a plain program's by a relative error of at most 0.011.
Values may be sent and summed in bfloat16 or wider, within the bound.
A program may use at most 64 MiB of HBM per device.

v0:
```python
import jax
import jax.numpy as jnp
from jax import lax
from jax.sharding import PartitionSpec as P

SEQS = 2


def in_blocks(x, dim, peers):
    before, after = (x.shape[:dim], x.shape[dim + 1 :])
    return jnp.moveaxis(x.reshape(*before, peers, -1, *after), dim, 0)


def sent_and_summed(x, axis, dim):
    tiles = in_blocks(x, dim, lax.axis_size(axis))
    arrived = lax.all_to_all(tiles, axis, split_axis=0, concat_axis=0, tiled=True)
    return arrived.astype(jnp.float32).sum(axis=0)


def copy_for_each(x, axis):
    copies = jnp.broadcast_to(x, (lax.axis_size(axis), *x.shape))
    return lax.all_to_all(copies, axis, split_axis=0, concat_axis=0, tiled=True)


def of_everyone(x, axis):
    return copy_for_each(x, axis).sum(axis=0)


def rotate(projected, position):
    half_width = projected.shape[-1] // 2
    inverse = 1.0 / 10000.0 ** jnp.linspace(0.0, 1.0, half_width, dtype=jnp.float32)
    angle = position[:, None] * inverse[None, :]
    cosine = jnp.cos(angle)[:, None, :]
    sine = jnp.sin(angle)[:, None, :]
    first = projected[..., :half_width]
    second = projected[..., half_width:]
    return jnp.concatenate(
        [first * cosine - second * sine, first * sine + second * cosine], axis=-1
    )


def on_device(
    layer_input, key_weight, value_weight, decay_exponent, query_new, key_new, value_new, norm_gain
):
    tok_count = layer_input.shape[0]
    head_local = decay_exponent.shape[0]
    key_width = key_weight.shape[1] // head_local
    value_width = value_weight.shape[1] // head_local
    seq_span = lax.axis_size("sp") // SEQS
    seq_length = tok_count * seq_span
    sp_place = lax.axis_index("sp")
    feature_block = lax.all_gather(layer_input, "tp", axis=1, tiled=True)
    key_proj = jnp.dot(feature_block, key_weight, preferred_element_type=jnp.float32)
    value_proj = jnp.dot(feature_block, value_weight, preferred_element_type=jnp.float32)
    position = (sp_place % seq_span * tok_count + jnp.arange(tok_count, dtype=jnp.int32)).astype(
        jnp.float32
    )
    keys = (
        rotate(key_proj.reshape(tok_count, head_local, key_width), position) * key_width ** (-0.5)
    ).astype(jnp.bfloat16)
    values = value_proj.astype(jnp.bfloat16).reshape(tok_count, head_local, value_width)
    distance = seq_length - 1.0 - position
    weighting = jnp.exp(decay_exponent[None, :] * distance[:, None])
    weighted = (keys.astype(jnp.float32) * weighting[:, :, None]).astype(jnp.bfloat16)
    local_state = jnp.einsum("thd,the->hde", weighted, values, preferred_element_type=jnp.float32)
    member = (jnp.arange(SEQS, dtype=jnp.int32) == sp_place // seq_span).astype(jnp.float32)
    state_terms = member[:, None, None, None] * local_state[None]
    final_rows = sent_and_summed(state_terms.astype(jnp.bfloat16), "sp", 2)
    state_cache = final_rows.astype(jnp.bfloat16)
    queries = query_new.astype(jnp.float32).reshape(SEQS, head_local, key_width)
    partial_read = jnp.einsum(
        "shd,shde->she", queries, state_terms, precision=lax.Precision.HIGHEST
    )
    carried = of_everyone(partial_read, "sp")
    keys_next = key_new.astype(jnp.float32).reshape(SEQS, head_local, key_width)
    values_next = value_new.astype(jnp.float32).reshape(SEQS, head_local, value_width)
    own_term = jnp.sum(queries * keys_next, axis=2)[:, :, None] * values_next
    mixed = jnp.exp(decay_exponent)[None, :, None] * carried + own_term
    normed = mixed * lax.rsqrt(jnp.mean(mixed * mixed, axis=2, keepdims=True) + 1e-06)
    normed = normed * norm_gain.reshape(head_local, value_width)[None, :, :]
    return (state_cache, normed.reshape(SEQS, head_local * value_width).astype(jnp.bfloat16))


def solution(mesh):
    in_specs = (
        P("sp", "tp"),
        P(None, "tp"),
        P(None, "tp"),
        P("tp"),
        P(None, "tp"),
        P(None, "tp"),
        P(None, "tp"),
        P("tp"),
    )
    out_specs = (P(None, "tp", "sp", None), P(None, "tp"))
    return jax.shard_map(
        on_device, mesh=mesh, in_specs=in_specs, out_specs=out_specs, check_vma=False
    )
```

profile of v0, /device:TPU:1, one launch (start us, length us, event | category | flops | bytes accessed | tf_op | source)
XLA Modules:
  0.0 174.9 jit_solution(16979299565072083331)
XLA Ops:
  7.2 0.0 copy-start
  7.2 0.0 all-gather.2.cloned.1.call-start
  7.2 0.7 all-gather.2.cloned.1.call-update
  7.9 0.7 reshape.155
  8.6 0.7 exp.11
  9.3 0.1 fusion.12
  9.4 0.7 convert_multiply_fusion
  10.1 0.7 multiply_exponential_fusion
  10.8 1.0 multiply_cosine_fusion
  11.8 95.6 %all-gather.2.cloned.1.call-done = bf16[1024,4096]{1,0:T(8,128)(2,1)} async-done(((bf16[1024,256]{1,0:T(8,128)(2,1)}), bf16[1024,4096]{1,0:T(8,128)(2,1)}) %all-gather.2.cloned.1.call-update) | async-done | bytes 8388624 | tf_op jit(solution)/shard_map/all_gather | solution.py:52
  107.5 0.0 copy-done
  107.5 0.0 copy-start.3
  107.5 5.9 %fusion.15 = f32[1024,256]{0,1:T(8,128)S(1)} fusion(bf16[1024,4096]{1,0:T(8,128)(2,1)} %all-gather.2.cloned.1.call-done, bf16[4096,256]{1,0:T(8,128)(2,1)S(1)} %copy-done), kind=kOutput, calls=%fused_computation.37 | convolution fusion | flops 2147483648 | bytes 11534336 | tf_op jit(solution)/shard_map/dot_general | solution.py:53
  113.4 0.0 copy-start.4
  113.4 0.2 multiply_subtract_fusion
  113.5 0.0 copy-done.3
  113.6 1.4 copy-done.4
  115.0 2.4 %convolution_convert_fusion = bf16[1024,256]{0,1:T(8,128)(2,1)S(1)} fusion(bf16[1024,4096]{1,0:T(8,128)(2,1)S(1)} %copy-done.3, bf16[4096,256]{1,0:T(8,128)(2,1)S(1)} %copy-done.4), kind=kOutput, calls=%fused_computation | convolution fusion | flops 2147745792 | bytes 11010048 | tf_op jit(solution)/shard_map/dot_general | solution.py:54
  117.4 0.0 copy-start.1
  117.4 0.0 copy-start.2
  117.4 0.3 fusion.1
  117.7 0.3 fusion.5
  118.0 0.6 broadcast_in_dim.4
  118.7 14.4 %all-to-all-start.1 = ((f32[32,2,2,128]{3,2,1,0:T(2,128)}), f32[32,2,2,128]{3,2,1,0:T(2,128)S(1)}, u32[]{:S(2)}, u32[]{:S(2)}) async-start(f32[32,2,2,128]{3,2,1,0:T(2,128)} %broadcast_in_dim.4), calls=%async_computation.1 | async-start | bytes 131072 | tf_op jit(solution)/shard_map/all_to_all | solution.py:22
  133.1 0.1 broadcast_bitcast_fusion.2
  133.1 0.0 copy-done.1
  133.2 0.1 reduce_sum.44
  133.2 0.8 multiply_convert_fusion.2
  134.0 12.1 %all-to-all-done.1 = f32[32,2,2,128]{3,2,1,0:T(2,128)S(1)} async-done(((f32[32,2,2,128]{3,2,1,0:T(2,128)}), f32[32,2,2,128]{3,2,1,0:T(2,128)S(1)}, u32[]{:S(2)}, u32[]{:S(2)}) %all-to-all-start.1) | async-done | bytes 65568 | tf_op jit(solution)/shard_map/all_to_all | solution.py:22
  146.1 5.1 %all-to-all-start = ((bf16[32,2,2,4,128]{4,3,2,1,0:T(4,128)(2,1)}), bf16[32,2,2,4,128]{4,3,2,1,0:T(4,128)(2,1)S(1)}, u32[]{:S(2)}, u32[]{:S(2)}) async-start(bf16[32,2,2,4,128]{4,3,2,1,0:T(4,128)(2,1)} %multiply_convert_fusion.2), calls=%async_computation | async-start | bytes 262144 | tf_op jit(solution)/shard_map/all_to_all | solution.py:16
  151.2 0.2 broadcast_bitcast_fusion.1
  151.4 0.1 broadcast_bitcast_fusion
  151.5 0.0 copy-done.2
  151.5 0.6 fusion.10
  152.0 15.3 %all-to-all-done = bf16[32,2,2,4,128]{4,3,2,1,0:T(4,128)(2,1)S(1)} async-done(((bf16[32,2,2,4,128]{4,3,2,1,0:T(4,128)(2,1)}), bf16[32,2,2,4,128]{4,3,2,1,0:T(4,128)(2,1)S(1)}, u32[]{:S(2)}, u32[]{:S(2)}) %all-to-all-start) | async-done | bytes 131104 | tf_op jit(solution)/shard_map/all_to_all | solution.py:16
  167.4 0.7 reduce_sum.41
  (8 shorter events, 0.1 us)
Async XLA Ops:
  7.2 100.3 %copy-start = (bf16[4096,256]{1,0:T(8,128)(2,1)S(1)}, bf16[4096,256]{1,0:T(8,128)(2,1)}, u32[]{:S(2)}) copy-start(bf16[4096,256]{1,0:T(8,128)(2,1)} %param.9) | copy-start | bytes 6291460
  7.2 100.3 %all-gather.2.cloned.1.call-start = ((), (), s32[]{:S(2)}) async-start(), calls=%async_computation.2 | async-start | bytes 8912896 | tf_op jit(solution)/shard_map/all_gather | solution.py:52
  107.5 6.1 %copy-start.3 = (bf16[1024,4096]{1,0:T(8,128)(2,1)S(1)}, bf16[1024,4096]{1,0:T(8,128)(2,1)}, u32[]{:S(2)}) copy-start(bf16[1024,4096]{1,0:T(8,128)(2,1)} %all-gather.2.cloned.1.call-done) | copy-start | bytes 25165828
  113.4 1.6 copy-start.4
  117.4 15.8 %copy-start.1 = (bf16[2,256]{1,0:T(2,128)(2,1)S(1)}, bf16[2,256]{1,0:T(2,128)(2,1)}, u32[]{:S(2)}) copy-start(bf16[2,256]{1,0:T(2,128)(2,1)} %param.14) | copy-start | bytes 3076
  117.4 34.1 %copy-start.2 = (f32[256]{0:T(256)S(1)}, f32[256]{0:T(256)}, u32[]{:S(2)}) copy-start(f32[256]{0:T(256)} %param.15) | copy-start | bytes 3076
  118.7 27.4 %all-to-all-start.1 = ((f32[32,2,2,128]{3,2,1,0:T(2,128)}), f32[32,2,2,128]{3,2,1,0:T(2,128)S(1)}, u32[]{:S(2)}, u32[]{:S(2)}) async-start(f32[32,2,2,128]{3,2,1,0:T(2,128)} %broadcast_in_dim.4), calls=%async_computation.1 | async-start | bytes 131072 | tf_op jit(solution)/shard_map/all_to_all | solution.py:22
  146.1 21.3 %all-to-all-start = ((bf16[32,2,2,4,128]{4,3,2,1,0:T(4,128)(2,1)}), bf16[32,2,2,4,128]{4,3,2,1,0:T(4,128)(2,1)S(1)}, u32[]{:S(2)}, u32[]{:S(2)}) async-start(bf16[32,2,2,4,128]{4,3,2,1,0:T(4,128)(2,1)} %multiply_convert_fusion.2), calls=%async_computation | async-start | bytes 262144 | tf_op jit(solution)/shard_map/all_to_all | solution.py:16
Sparse Core Ops, SparseCore 0:
  11.0 96.4 all-gather.1
where the time goes:
time: 175 us
  waiting for transfers between devices  124 us (71%)
  starting transfers between devices  19.5 us (11%)
  between operations  14.2 us (8%)
  matrix products  8.92 us (5%)
  other arithmetic  4.99 us (3%)
  local copies, waits for them, and re-layouts  3.61 us (2%)
    all_gather x1, waiting for transfers between devices, on_device(): feature_block = lax.all_gather(layer_input, 'tp', axis=1, tiled=True)  95.6 us
    all_to_all x1, waiting for transfers between devices, sent_and_summed(): lax.all_to_all(tiles, axis, split_axis=0, concat_axis=0, tiled=True)  15.3 us
    all_to_all x1, starting transfers between devices, copy_for_each(): return lax.all_to_all(copies, axis, split_axis=0, concat_axis=0, tiled=True)  14.4 us
    all_to_all x1, waiting for transfers between devices, copy_for_each(): return lax.all_to_all(copies, axis, split_axis=0, concat_axis=0, tiled=True)  12.1 us
    dot_general x1, matrix products, on_device(): jnp.dot(feature_block, key_weight, preferred_element_type=jnp.float32)  5.9 us
    all_to_all x1, starting transfers between devices, sent_and_summed(): lax.all_to_all(tiles, axis, split_axis=0, concat_axis=0, tiled=True)  5.1 us
  transfers between devices with their start and end apart: 3, of which 3 were waited for; matrix products, arithmetic and copies ran while one was open for 3% of the time, Pallas kernels for 0%

commit v1 on v0

--- a/solution.py
+++ b/solution.py
@@ -49,7 +49,26 @@
     seq_span = lax.axis_size("sp") // SEQS
     seq_length = tok_count * seq_span
     sp_place = lax.axis_index("sp")
-    feature_block = lax.all_gather(layer_input, "tp", axis=1, tiled=True)
+    size, index, span = (lax.axis_size("tp"), lax.axis_index("tp"), layer_input.shape[1])
+    upward = [(i, (i + 1) % size) for i in range(size)]
+    downward = [(i, (i - 1) % size) for i in range(size)]
+    filled = jnp.zeros(
+        (*layer_input.shape[:1], size * span, *layer_input.shape[1 + 1 :]), layer_input.dtype
+    )
+    filled = lax.dynamic_update_slice_in_dim(filled, layer_input, index * span, axis=1)
+    from_left = from_right = layer_input
+    half = size // 2
+    for lap in range(1, half + 1):
+        from_left = lax.ppermute(from_left, "tp", upward)
+        filled = lax.dynamic_update_slice_in_dim(
+            filled, from_left, (index - lap) % size * span, axis=1
+        )
+        if lap < size - half:
+            from_right = lax.ppermute(from_right, "tp", downward)
+            filled = lax.dynamic_update_slice_in_dim(
+                filled, from_right, (index + lap) % size * span, axis=1
+            )
+    feature_block = filled
     key_proj = jnp.dot(feature_block, key_weight, preferred_element_type=jnp.float32)
     value_proj = jnp.dot(feature_block, value_weight, preferred_element_type=jnp.float32)
     position = (sp_place % seq_span * tok_count + jnp.arange(tok_count, dtype=jnp.int32)).astype(

time: 175 us -> 206 us (1.18)
  starting transfers between devices: 19.5 us -> 105 us
  waiting for transfers between devices: 124 us -> 51 us
  local copies, waits for them, and re-layouts: 3.61 us -> 29.8 us
  between operations: 14.2 us -> 1.31 us
  matrix products: 8.92 us -> 12.3 us
    all_gather x1 -> x0, waiting for transfers between devices: 95.6 us -> none  [on_device(): feature_block = lax.all_gather(layer_input, 'tp', axis=1, tiled=True)]
    ppermute x0 -> x15, starting transfers between devices: none -> 65.7 us  [the longest x7 45.6 us: on_device(): from_right = lax.ppermute(from_right, 'tp', downward)]
    dynamic_update_slice x0 -> x16, local copies, waits for them, and re-layouts: none -> 24.6 us  [the longest x8 12.3 us: on_device(): lax.dynamic_update_slice_in_dim(filled, from_left, (index - lap) % size *...]
    ppermute x0 -> x15, waiting for transfers between devices: none -> 23.6 us  [the longest x8 23.5 us: on_device(): from_left = lax.ppermute(from_left, 'tp', upward)]
    all_to_all x1, starting transfers between devices: 14.4 us -> 34.5 us  [copy_for_each(): return lax.all_to_all(copies, axis, split_axis=0, concat_axis=0, tiled=True)]
    broadcast_in_dim x0 -> x1, local copies, waits for them, and re-layouts: none -> 4.29 us  [on_device(): jnp.zeros((*layer_input.shape[:1], size * span, *layer_input.shape[1 + 1:...]
    dot_general x1, matrix products: 2.41 us -> 5.78 us  [on_device(): jnp.dot(feature_block, value_weight, preferred_element_type=jnp.float32)]
  transfers between devices with their start and end apart: 3 -> 17, of which waited for: 3 -> 8; matrix products, arithmetic and copies ran while one was open for 3% -> 16% of each run, Pallas kernels for 0% -> 0%
where the time goes in v1:
time: 206 us; the launch traced here: 205 us
  starting transfers between devices  105 us (51%)
  waiting for transfers between devices  51 us (25%)
  local copies, waits for them, and re-layouts  29.8 us (14%)
  matrix products  12.3 us (6%)
  other arithmetic  5 us (2%)
    ppermute x7, starting transfers between devices, on_device(): from_right = lax.ppermute(from_right, 'tp', downward)  45.6 us
    all_to_all x1, starting transfers between devices, copy_for_each(): return lax.all_to_all(copies, axis, split_axis=0, concat_axis=0, tiled=True)  34.5 us
    ppermute x8, waiting for transfers between devices, on_device(): from_left = lax.ppermute(from_left, 'tp', upward)  23.5 us
    ppermute x8, starting transfers between devices, on_device(): from_left = lax.ppermute(from_left, 'tp', upward)  20 us
    all_to_all x1, waiting for transfers between devices, sent_and_summed(): lax.all_to_all(tiles, axis, split_axis=0, concat_axis=0, tiled=True)  15.3 us
    dynamic_update_slice x8, local copies, waits for them, and re-layouts, on_device(): lax.dynamic_update_slice_in_dim(filled, from_left, (index - lap) % size *...  12.3 us
    all_to_all x1, waiting for transfers between devices, copy_for_each(): return lax.all_to_all(copies, axis, split_axis=0, concat_axis=0, tiled=True)  12.1 us
    dynamic_update_slice x7, local copies, waits for them, and re-layouts, on_device(): lax.dynamic_update_slice_in_dim(filled, from_right, (index + lap) % size...  11.4 us
  transfers between devices with their start and end apart: 17, of which 8 were waited for; matrix products, arithmetic and copies ran while one was open for 16% of the time, Pallas kernels for 0%

profile of v1, /device:TPU:1, one launch (start us, length us, event | category | flops | bytes accessed | tf_op | source)
XLA Modules:
  0.0 204.6 jit_solution(9694322404143259579)
XLA Ops:
  0.7 4.1 %collective-permute-start = (bf16[1024,256]{1,0:T(8,128)(2,1)}, bf16[1024,256]{1,0:T(8,128)(2,1)S(1)}, u32[]{:S(2)}, u32[]{:S(2)}) collective-permute-start(bf16[1024,256]{1,0:T(8,128)(2,1)} %param.8), channel_id=1, source_target_pairs={{0,1},{1,2},{2,3},{3,4},{4,5},{5,6},{6,7},{7,8},{8,9},{9,10},{10,1... | collective-permute-start | bytes 1572872 | tf_op jit(solution)/shard_map/ppermute | solution.py:62
  4.8 5.6 %collective-permute-start.1 = (bf16[1024,256]{1,0:T(8,128)(2,1)}, bf16[1024,256]{1,0:T(8,128)(2,1)}, u32[]{:S(2)}, u32[]{:S(2)}) collective-permute-start(bf16[1024,256]{1,0:T(8,128)(2,1)} %param.8), channel_id=1, source_target_pairs={{0,15},{1,0},{2,1},{3,2},{4,3},{5,4},{6,5},{7,6},{8,7},{9,8},{10,9... | collective-permute-start | bytes 1572872 | tf_op jit(solution)/shard_map/ppermute | solution.py:67
  10.4 4.8 %collective-permute-done = bf16[1024,256]{1,0:T(8,128)(2,1)S(1)} collective-permute-done((bf16[1024,256]{1,0:T(8,128)(2,1)}, bf16[1024,256]{1,0:T(8,128)(2,1)S(1)}, u32[]{:S(2)}, u32[]{:S(2)}) %collective-permute-start) | collective-permute-done | bytes 524320 | tf_op jit(solution)/shard_map/ppermute | solution.py:62
  15.2 3.5 %collective-permute-start.2 = (bf16[1024,256]{1,0:T(8,128)(2,1)S(1)}, bf16[1024,256]{1,0:T(8,128)(2,1)}, u32[]{:S(2)}, u32[]{:S(2)}) collective-permute-start(bf16[1024,256]{1,0:T(8,128)(2,1)S(1)} %collective-permute-done), channel_id=1, source_target_pairs={{0,1},{1,2},{2,3},{3,4},{4,5},{5,6},{6,7},{7,8},{8,9},{9,10},{10,1... | collective-permute-start | bytes 1572872 | tf_op jit(solution)/shard_map/ppermute | solution.py:62
  18.8 6.5 %collective-permute-start.3 = (bf16[1024,256]{1,0:T(8,128)(2,1)}, bf16[1024,256]{1,0:T(8,128)(2,1)}, u32[]{:S(2)}, u32[]{:S(2)}) collective-permute-start(bf16[1024,256]{1,0:T(8,128)(2,1)} %collective-permute-done.1), channel_id=1, source_target_pairs={{0,15},{1,0},{2,1},{3,2},{4,3},{5,4},{6,5},{7,6},{8,7},{9,8},{10,9... | collective-permute-start | bytes 1572872 | tf_op jit(solution)/shard_map/ppermute | solution.py:67
  25.3 4.7 %collective-permute-done.2 = bf16[1024,256]{1,0:T(8,128)(2,1)} collective-permute-done((bf16[1024,256]{1,0:T(8,128)(2,1)S(1)}, bf16[1024,256]{1,0:T(8,128)(2,1)}, u32[]{:S(2)}, u32[]{:S(2)}) %collective-permute-start.2) | collective-permute-done | bytes 524320 | tf_op jit(solution)/shard_map/ppermute | solution.py:62
  30.0 2.7 %collective-permute-start.4 = (bf16[1024,256]{1,0:T(8,128)(2,1)}, bf16[1024,256]{1,0:T(8,128)(2,1)S(1)}, u32[]{:S(2)}, u32[]{:S(2)}) collective-permute-start(bf16[1024,256]{1,0:T(8,128)(2,1)} %collective-permute-done.2), channel_id=1, source_target_pairs={{0,1},{1,2},{2,3},{3,4},{4,5},{5,6},{6,7},{7,8},{8,9},{9,10},{10,1... | collective-permute-start | bytes 1572872 | tf_op jit(solution)/shard_map/ppermute | solution.py:62
  32.7 6.5 %collective-permute-start.5 = (bf16[1024,256]{1,0:T(8,128)(2,1)}, bf16[1024,256]{1,0:T(8,128)(2,1)}, u32[]{:S(2)}, u32[]{:S(2)}) collective-permute-start(bf16[1024,256]{1,0:T(8,128)(2,1)} %collective-permute-done.3), channel_id=1, source_target_pairs={{0,15},{1,0},{2,1},{3,2},{4,3},{5,4},{6,5},{7,6},{8,7},{9,8},{10,9... | collective-permute-start | bytes 1572872 | tf_op jit(solution)/shard_map/ppermute | solution.py:67
  39.3 4.8 %collective-permute-done.4 = bf16[1024,256]{1,0:T(8,128)(2,1)S(1)} collective-permute-done((bf16[1024,256]{1,0:T(8,128)(2,1)}, bf16[1024,256]{1,0:T(8,128)(2,1)S(1)}, u32[]{:S(2)}, u32[]{:S(2)}) %collective-permute-start.4) | collective-permute-done | bytes 524320 | tf_op jit(solution)/shard_map/ppermute | solution.py:62
  44.1 2.1 %collective-permute-start.6 = (bf16[1024,256]{1,0:T(8,128)(2,1)S(1)}, bf16[1024,256]{1,0:T(8,128)(2,1)}, u32[]{:S(2)}, u32[]{:S(2)}) collective-permute-start(bf16[1024,256]{1,0:T(8,128)(2,1)S(1)} %collective-permute-done.4), channel_id=1, source_target_pairs={{0,1},{1,2},{2,3},{3,4},{4,5},{5,6},{6,7},{7,8},{8,9},{9,10},{10,1... | collective-permute-start | bytes 1572872 | tf_op jit(solution)/shard_map/ppermute | solution.py:62
  46.2 0.7 convert_multiply_fusion
  46.9 0.7 multiply_exponential_fusion
  47.7 6.5 %collective-permute-start.7 = (bf16[1024,256]{1,0:T(8,128)(2,1)}, bf16[1024,256]{1,0:T(8,128)(2,1)}, u32[]{:S(2)}, u32[]{:S(2)}) collective-permute-start(bf16[1024,256]{1,0:T(8,128)(2,1)} %collective-permute-done.5), channel_id=1, source_target_pairs={{0,15},{1,0},{2,1},{3,2},{4,3},{5,4},{6,5},{7,6},{8,7},{9,8},{10,9... | collective-permute-start | bytes 1572872 | tf_op jit(solution)/shard_map/ppermute | solution.py:67
  54.2 3.3 %collective-permute-done.6 = bf16[1024,256]{1,0:T(8,128)(2,1)} collective-permute-done((bf16[1024,256]{1,0:T(8,128)(2,1)S(1)}, bf16[1024,256]{1,0:T(8,128)(2,1)}, u32[]{:S(2)}, u32[]{:S(2)}) %collective-permute-start.6) | collective-permute-done | bytes 524320 | tf_op jit(solution)/shard_map/ppermute | solution.py:62
  57.4 1.9 collective-permute-start.8
  59.4 1.0 multiply_cosine_fusion
  60.6 7.1 %collective-permute-start.9 = (bf16[1024,256]{1,0:T(8,128)(2,1)}, bf16[1024,256]{1,0:T(8,128)(2,1)}, u32[]{:S(2)}, u32[]{:S(2)}) collective-permute-start(bf16[1024,256]{1,0:T(8,128)(2,1)} %collective-permute-done.7), channel_id=1, source_target_pairs={{0,15},{1,0},{2,1},{3,2},{4,3},{5,4},{6,5},{7,6},{8,7},{9,8},{10,9... | collective-permute-start | bytes 1572872 | tf_op jit(solution)/shard_map/ppermute | solution.py:67
  67.7 4.3 %broadcast_in_dim.6 = bf16[1024,4096]{1,0:T(8,128)(2,1)} broadcast(bf16[]{:T(256)} %constant.131.clone.1), dimensions={} | broadcast | bytes 8388610 | tf_op jit(solution)/shard_map/broadcast_in_dim | solution.py:55
  72.0 0.9 constant_dynamic-update-slice_fusion.15
  72.9 1.9 collective-permute-start.10
  75.2 1.9 constant_dynamic-update-slice_fusion.14
  77.1 1.9 constant_dynamic-update-slice_fusion.13
  79.0 2.0 constant_dynamic-update-slice_fusion.12
  81.0 6.7 %collective-permute-start.11 = (bf16[1024,256]{1,0:T(8,128)(2,1)}, bf16[1024,256]{1,0:T(8,128)(2,1)S(1)}, u32[]{:S(2)}, u32[]{:S(2)}) collective-permute-start(bf16[1024,256]{1,0:T(8,128)(2,1)} %collective-permute-done.9), channel_id=1, source_target_pairs={{0,15},{1,0},{2,1},{3,2},{4,3},{5,4},{6,5},{7,6},{8,7},{9,8},{10,9... | collective-permute-start | bytes 1572872 | tf_op jit(solution)/shard_map/ppermute | solution.py:67
  87.7 1.9 constant_dynamic-update-slice_fusion.11
  89.6 1.9 collective-permute-start.12
  91.5 1.9 constant_dynamic-update-slice_fusion.10
  93.5 1.9 constant_dynamic-update-slice_fusion.9
  95.4 1.9 constant_dynamic-update-slice_fusion.8
  97.3 1.9 constant_dynamic-update-slice_fusion.7
  99.3 6.7 %collective-permute-start.13 = (bf16[1024,256]{1,0:T(8,128)(2,1)S(1)}, bf16[1024,256]{1,0:T(8,128)(2,1)S(1)}, u32[]{:S(2)}, u32[]{:S(2)}) collective-permute-start(bf16[1024,256]{1,0:T(8,128)(2,1)S(1)} %collective-permute-done.11), channel_id=1, source_target_pairs={{0,15},{1,0},{2,1},{3,2},{4,3},{5,4},{6,5},{7,6},{8,7},{9,8},{10,9... | collective-permute-start | bytes 1572872 | tf_op jit(solution)/shard_map/ppermute | solution.py:67
  105.9 1.9 constant_dynamic-update-slice_fusion.6
  107.9 1.9 collective-permute-start.14
  109.8 1.9 constant_dynamic-update-slice_fusion.5
  111.7 0.9 constant_dynamic-update-slice_fusion.4
  112.6 0.9 constant_dynamic-update-slice_fusion.3
  113.5 0.9 constant_dynamic-update-slice_fusion.2
  114.3 0.9 constant_dynamic-update-slice_fusion.1
  115.2 5.9 %collective-permute-done.14 = bf16[1024,256]{1,0:T(8,128)(2,1)S(1)} collective-permute-done((bf16[1024,256]{1,0:T(8,128)(2,1)S(1)}, bf16[1024,256]{1,0:T(8,128)(2,1)S(1)}, u32[]{:S(2)}, u32[]{:S(2)}) %collective-permute-start.14) | collective-permute-done | bytes 524320 | tf_op jit(solution)/shard_map/ppermute | solution.py:62
  121.1 0.9 constant_dynamic-update-slice_fusion
  122.0 5.9 %fusion.15 = f32[1024,256]{0,1:T(8,128)S(1)} fusion(bf16[1024,4096]{1,0:T(8,128)(2,1)} %constant_dynamic-update-slice_fusion, bf16[4096,256]{1,0:T(8,128)(2,1)S(1)} %copy-done), kind=kOutput, calls=%fused_computation.53 | convolution fusion | flops 2147483648 | bytes 11534336 | tf_op jit(solution)/shard_map/dot_general | solution.py:72
  127.9 5.8 %convolution_convert_fusion = bf16[1024,256]{0,1:T(8,128)(2,1)S(1)} fusion(bf16[1024,4096]{1,0:T(8,128)(2,1)} %constant_dynamic-update-slice_fusion, bf16[4096,256]{1,0:T(8,128)(2,1)S(1)} %copy-done.8), kind=kOutput, calls=%fused_computation | convolution fusion | flops 2147745792 | bytes 11010048 | tf_op jit(solution)/shard_map/dot_general | solution.py:73
  135.2 34.5 %all-to-all-start.1 = ((f32[32,2,2,128]{3,2,1,0:T(2,128)}), f32[32,2,2,128]{3,2,1,0:T(2,128)S(1)}, u32[]{:S(2)}, u32[]{:S(2)}) async-start(f32[32,2,2,128]{3,2,1,0:T(2,128)} %broadcast_in_dim.7), calls=%async_computation.1 | async-start | bytes 131072 | tf_op jit(solution)/shard_map/all_to_all | solution.py:22
  169.8 0.8 multiply_convert_fusion.2
  170.6 12.1 %all-to-all-done.1 = f32[32,2,2,128]{3,2,1,0:T(2,128)S(1)} async-done(((f32[32,2,2,128]{3,2,1,0:T(2,128)}), f32[32,2,2,128]{3,2,1,0:T(2,128)S(1)}, u32[]{:S(2)}, u32[]{:S(2)}) %all-to-all-start.1) | async-done | bytes 65568 | tf_op jit(solution)/shard_map/all_to_all | solution.py:22
  182.6 5.1 %all-to-all-start = ((bf16[32,2,2,4,128]{4,3,2,1,0:T(4,128)(2,1)}), bf16[32,2,2,4,128]{4,3,2,1,0:T(4,128)(2,1)S(1)}, u32[]{:S(2)}, u32[]{:S(2)}) async-start(bf16[32,2,2,4,128]{4,3,2,1,0:T(4,128)(2,1)} %multiply_convert_fusion.2), calls=%async_computation | async-start | bytes 262144 | tf_op jit(solution)/shard_map/all_to_all | solution.py:16
  188.6 15.3 %all-to-all-done = bf16[32,2,2,4,128]{4,3,2,1,0:T(4,128)(2,1)S(1)} async-done(((bf16[32,2,2,4,128]{4,3,2,1,0:T(4,128)(2,1)}), bf16[32,2,2,4,128]{4,3,2,1,0:T(4,128)(2,1)S(1)}, u32[]{:S(2)}, u32[]{:S(2)}) %all-to-all-start) | async-done | bytes 131104 | tf_op jit(solution)/shard_map/all_to_all | solution.py:16
  204.0 0.7 reduce_sum.41
  (48 shorter events, 2.8 us)
Async XLA Ops:
  0.6 121.4 %copy-start = (bf16[4096,256]{1,0:T(8,128)(2,1)S(1)}, bf16[4096,256]{1,0:T(8,128)(2,1)}, u32[]{:S(2)}) copy-start(bf16[4096,256]{1,0:T(8,128)(2,1)} %param.9) | copy-start | bytes 6291460
  0.6 71.3 %copy-start.1 = (bf16[1024,256]{1,0:T(8,128)(2,1)S(1)}, bf16[1024,256]{1,0:T(8,128)(2,1)}, u32[]{:S(2)}) copy-start(bf16[1024,256]{1,0:T(8,128)(2,1)} %param.8) | copy-start | bytes 1572868
  0.7 74.4 %copy-start.5 = (bf16[2,256]{1,0:T(2,128)(2,1)S(1)}, bf16[2,256]{1,0:T(2,128)(2,1)}, u32[]{:S(2)}) copy-start(bf16[2,256]{1,0:T(2,128)(2,1)} %param.12) | copy-start | bytes 3076
  0.7 74.4 %copy-start.7 = (f32[2]{0:T(128)S(1)}, f32[2]{0:T(128)}, u32[]{:S(2)}) copy-start(f32[2]{0:T(128)} %param.11) | copy-start | bytes 28
  0.7 14.6 %collective-permute-start = (bf16[1024,256]{1,0:T(8,128)(2,1)}, bf16[1024,256]{1,0:T(8,128)(2,1)S(1)}, u32[]{:S(2)}, u32[]{:S(2)}) collective-permute-start(bf16[1024,256]{1,0:T(8,128)(2,1)} %param.8), channel_id=1, source_target_pairs={{0,1},{1,2},{2,3},{3,4},{4,5},{5,6},{6,7},{7,8},{8,9},{9,10},{10,1... | collective-permute-start | bytes 1572872 | tf_op jit(solution)/shard_map/ppermute | solution.py:62
  4.8 14.0 %collective-permute-start.1 = (bf16[1024,256]{1,0:T(8,128)(2,1)}, bf16[1024,256]{1,0:T(8,128)(2,1)}, u32[]{:S(2)}, u32[]{:S(2)}) collective-permute-start(bf16[1024,256]{1,0:T(8,128)(2,1)} %param.8), channel_id=1, source_target_pairs={{0,15},{1,0},{2,1},{3,2},{4,3},{5,4},{6,5},{7,6},{8,7},{9,8},{10,9... | collective-permute-start | bytes 1572872 | tf_op jit(solution)/shard_map/ppermute | solution.py:67
  15.2 10.1 %copy-start.3 = (bf16[1024,256]{1,0:T(8,128)(2,1)}, bf16[1024,256]{1,0:T(8,128)(2,1)S(1)}, u32[]{:S(2)}) copy-start(bf16[1024,256]{1,0:T(8,128)(2,1)S(1)} %collective-permute-done) | copy-start | bytes 1572868
  15.2 14.8 %collective-permute-start.2 = (bf16[1024,256]{1,0:T(8,128)(2,1)S(1)}, bf16[1024,256]{1,0:T(8,128)(2,1)}, u32[]{:S(2)}, u32[]{:S(2)}) collective-permute-start(bf16[1024,256]{1,0:T(8,128)(2,1)S(1)} %collective-permute-done), channel_id=1, source_target_pairs={{0,1},{1,2},{2,3},{3,4},{4,5},{5,6},{6,7},{7,8},{8,9},{9,10},{10,1... | collective-permute-start | bytes 1572872 | tf_op jit(solution)/shard_map/ppermute | solution.py:62
  18.8 13.9 %collective-permute-start.3 = (bf16[1024,256]{1,0:T(8,128)(2,1)}, bf16[1024,256]{1,0:T(8,128)(2,1)}, u32[]{:S(2)}, u32[]{:S(2)}) collective-permute-start(bf16[1024,256]{1,0:T(8,128)(2,1)} %collective-permute-done.1), channel_id=1, source_target_pairs={{0,15},{1,0},{2,1},{3,2},{4,3},{5,4},{6,5},{7,6},{8,7},{9,8},{10,9... | collective-permute-start | bytes 1572872 | tf_op jit(solution)/shard_map/ppermute | solution.py:67
  30.0 14.0 %collective-permute-start.4 = (bf16[1024,256]{1,0:T(8,128)(2,1)}, bf16[1024,256]{1,0:T(8,128)(2,1)S(1)}, u32[]{:S(2)}, u32[]{:S(2)}) collective-permute-start(bf16[1024,256]{1,0:T(8,128)(2,1)} %collective-permute-done.2), channel_id=1, source_target_pairs={{0,1},{1,2},{2,3},{3,4},{4,5},{5,6},{6,7},{7,8},{8,9},{9,10},{10,1... | collective-permute-start | bytes 1572872 | tf_op jit(solution)/shard_map/ppermute | solution.py:62
  32.7 14.9 %collective-permute-start.5 = (bf16[1024,256]{1,0:T(8,128)(2,1)}, bf16[1024,256]{1,0:T(8,128)(2,1)}, u32[]{:S(2)}, u32[]{:S(2)}) collective-permute-start(bf16[1024,256]{1,0:T(8,128)(2,1)} %collective-permute-done.3), channel_id=1, source_target_pairs={{0,15},{1,0},{2,1},{3,2},{4,3},{5,4},{6,5},{7,6},{8,7},{9,8},{10,9... | collective-permute-start | bytes 1572872 | tf_op jit(solution)/shard_map/ppermute | solution.py:67
  44.1 15.3 %copy-start.2 = (bf16[1024,256]{1,0:T(8,128)(2,1)}, bf16[1024,256]{1,0:T(8,128)(2,1)S(1)}, u32[]{:S(2)}) copy-start(bf16[1024,256]{1,0:T(8,128)(2,1)S(1)} %collective-permute-done.4) | copy-start | bytes 1572868
  44.1 13.3 %collective-permute-start.6 = (bf16[1024,256]{1,0:T(8,128)(2,1)S(1)}, bf16[1024,256]{1,0:T(8,128)(2,1)}, u32[]{:S(2)}, u32[]{:S(2)}) collective-permute-start(bf16[1024,256]{1,0:T(8,128)(2,1)S(1)} %collective-permute-done.4), channel_id=1, source_target_pairs={{0,1},{1,2},{2,3},{3,4},{4,5},{5,6},{6,7},{7,8},{8,9},{9,10},{10,1... | collective-permute-start | bytes 1572872 | tf_op jit(solution)/shard_map/ppermute | solution.py:62
  47.7 12.9 %collective-permute-start.7 = (bf16[1024,256]{1,0:T(8,128)(2,1)}, bf16[1024,256]{1,0:T(8,128)(2,1)}, u32[]{:S(2)}, u32[]{:S(2)}) collective-permute-start(bf16[1024,256]{1,0:T(8,128)(2,1)} %collective-permute-done.5), channel_id=1, source_target_pairs={{0,15},{1,0},{2,1},{3,2},{4,3},{5,4},{6,5},{7,6},{8,7},{9,8},{10,9... | collective-permute-start | bytes 1572872 | tf_op jit(solution)/shard_map/ppermute | solution.py:67
  57.4 15.4 %collective-permute-start.8 = (bf16[1024,256]{1,0:T(8,128)(2,1)}, bf16[1024,256]{1,0:T(8,128)(2,1)}, u32[]{:S(2)}, u32[]{:S(2)}) collective-permute-start(bf16[1024,256]{1,0:T(8,128)(2,1)} %collective-permute-done.6), channel_id=1, source_target_pairs={{0,1},{1,2},{2,3},{3,4},{4,5},{5,6},{6,7},{7,8},{8,9},{9,10},{10,1... | collective-permute-start | bytes 1572872 | tf_op jit(solution)/shard_map/ppermute | solution.py:62
  60.6 20.4 %collective-permute-start.9 = (bf16[1024,256]{1,0:T(8,128)(2,1)}, bf16[1024,256]{1,0:T(8,128)(2,1)}, u32[]{:S(2)}, u32[]{:S(2)}) collective-permute-start(bf16[1024,256]{1,0:T(8,128)(2,1)} %collective-permute-done.7), channel_id=1, source_target_pairs={{0,15},{1,0},{2,1},{3,2},{4,3},{5,4},{6,5},{7,6},{8,7},{9,8},{10,9... | collective-permute-start | bytes 1572872 | tf_op jit(solution)/shard_map/ppermute | solution.py:67
  72.9 16.8 %collective-permute-start.10 = (bf16[1024,256]{1,0:T(8,128)(2,1)}, bf16[1024,256]{1,0:T(8,128)(2,1)S(1)}, u32[]{:S(2)}, u32[]{:S(2)}) collective-permute-start(bf16[1024,256]{1,0:T(8,128)(2,1)} %collective-permute-done.8), channel_id=1, source_target_pairs={{0,1},{1,2},{2,3},{3,4},{4,5},{5,6},{6,7},{7,8},{8,9},{9,10},{10,1... | collective-permute-start | bytes 1572872 | tf_op jit(solution)/shard_map/ppermute | solution.py:62
  81.0 18.3 %collective-permute-start.11 = (bf16[1024,256]{1,0:T(8,128)(2,1)}, bf16[1024,256]{1,0:T(8,128)(2,1)S(1)}, u32[]{:S(2)}, u32[]{:S(2)}) collective-permute-start(bf16[1024,256]{1,0:T(8,128)(2,1)} %collective-permute-done.9), channel_id=1, source_target_pairs={{0,15},{1,0},{2,1},{3,2},{4,3},{5,4},{6,5},{7,6},{8,7},{9,8},{10,9... | collective-permute-start | bytes 1572872 | tf_op jit(solution)/shard_map/ppermute | solution.py:67
  89.6 18.2 %collective-permute-start.12 = (bf16[1024,256]{1,0:T(8,128)(2,1)S(1)}, bf16[1024,256]{1,0:T(8,128)(2,1)S(1)}, u32[]{:S(2)}, u32[]{:S(2)}) collective-permute-start(bf16[1024,256]{1,0:T(8,128)(2,1)S(1)} %collective-permute-done.10), channel_id=1, source_target_pairs={{0,1},{1,2},{2,3},{3,4},{4,5},{5,6},{6,7},{7,8},{8,9},{9,10},{10,1... | collective-permute-start | bytes 1572872 | tf_op jit(solution)/shard_map/ppermute | solution.py:62
  99.3 15.1 %collective-permute-start.13 = (bf16[1024,256]{1,0:T(8,128)(2,1)S(1)}, bf16[1024,256]{1,0:T(8,128)(2,1)S(1)}, u32[]{:S(2)}, u32[]{:S(2)}) collective-permute-start(bf16[1024,256]{1,0:T(8,128)(2,1)S(1)} %collective-permute-done.11), channel_id=1, source_target_pairs={{0,15},{1,0},{2,1},{3,2},{4,3},{5,4},{6,5},{7,6},{8,7},{9,8},{10,9... | collective-permute-start | bytes 1572872 | tf_op jit(solution)/shard_map/ppermute | solution.py:67
  107.9 13.2 %collective-permute-start.14 = (bf16[1024,256]{1,0:T(8,128)(2,1)S(1)}, bf16[1024,256]{1,0:T(8,128)(2,1)S(1)}, u32[]{:S(2)}, u32[]{:S(2)}) collective-permute-start(bf16[1024,256]{1,0:T(8,128)(2,1)S(1)} %collective-permute-done.12), channel_id=1, source_target_pairs={{0,1},{1,2},{2,3},{3,4},{4,5},{5,6},{6,7},{7,8},{8,9},{9,10},{10,1... | collective-permute-start | bytes 1572872 | tf_op jit(solution)/shard_map/ppermute | solution.py:62
  122.0 5.9 %copy-start.8 = (bf16[4096,256]{1,0:T(8,128)(2,1)S(1)}, bf16[4096,256]{1,0:T(8,128)(2,1)}, u32[]{:S(2)}) copy-start(bf16[4096,256]{1,0:T(8,128)(2,1)} %param.10) | copy-start | bytes 6291460
  127.9 41.8 %copy-start.4 = (bf16[2,256]{1,0:T(2,128)(2,1)S(1)}, bf16[2,256]{1,0:T(2,128)(2,1)}, u32[]{:S(2)}) copy-start(bf16[2,256]{1,0:T(2,128)(2,1)} %param.14) | copy-start | bytes 3076
  127.9 60.1 %copy-start.6 = (f32[256]{0:T(256)S(1)}, f32[256]{0:T(256)}, u32[]{:S(2)}) copy-start(f32[256]{0:T(256)} %param.15) | copy-start | bytes 3076
  135.2 47.5 %all-to-all-start.1 = ((f32[32,2,2,128]{3,2,1,0:T(2,128)}), f32[32,2,2,128]{3,2,1,0:T(2,128)S(1)}, u32[]{:S(2)}, u32[]{:S(2)}) async-start(f32[32,2,2,128]{3,2,1,0:T(2,128)} %broadcast_in_dim.7), calls=%async_computation.1 | async-start | bytes 131072 | tf_op jit(solution)/shard_map/all_to_all | solution.py:22
  182.6 21.3 %all-to-all-start = ((bf16[32,2,2,4,128]{4,3,2,1,0:T(4,128)(2,1)}), bf16[32,2,2,4,128]{4,3,2,1,0:T(4,128)(2,1)S(1)}, u32[]{:S(2)}, u32[]{:S(2)}) async-start(bf16[32,2,2,4,128]{4,3,2,1,0:T(4,128)(2,1)} %multiply_convert_fusion.2), calls=%async_computation | async-start | bytes 262144 | tf_op jit(solution)/shard_map/all_to_all | solution.py:16
